TPU v7x, 512 devices: a 8x2x16 block of a 8x16x16 slice. The times are simulated.
512 devices in a mesh: grp: 2 (over y), kv: 16 (over z), tp: 16 (over x, core).
Axes of the slice: x: 8, y: 2, z: 16, core: 2. Of those that a mesh axis runs over, the one named last changes fastest.
The devices are a block of a 8x16x16 slice.
Arguments:
- tokens: bfloat16 [640, 4096], P('grp', ('kv', 'tp')), parts along dimension 0, may hold values from -65 to 65
- lengths: int32 [640], P(('grp', 'kv')), parts along dimension 0, may hold values from 1 to 16384, 1310720 in all
- memory: float32 [640, 16, 128, 128], P(('grp', 'kv'), 'tp'), parts along dimension 0, may hold values from -6 to 6
- norm_attn: bfloat16 [4096], P('kv'), may hold values from 0.099609375 to 1.8984375
- w_query: bfloat16 [4096, 2048], P('kv', 'tp'), may hold values from -0.09375 to 0.09375
- w_key: bfloat16 [4096, 2048], P('kv', 'tp'), may hold values from -0.09375 to 0.09375
- w_value: bfloat16 [4096, 2048], P('kv', 'tp'), may hold values from -0.09375 to 0.09375
- w_gate: bfloat16 [4096, 2048], P('kv', 'tp'), may hold values from -0.09375 to 0.09375
- head_gain: bfloat16 [2048], P('tp'), may hold values from 0.099609375 to 1.8984375
- w_out: bfloat16 [2048, 4096], P('tp', 'kv'), may hold values from -0.1875 to 0.1875
- norm_mlp: bfloat16 [4096], P('kv'), may hold values from 0.099609375 to 1.8984375
- w_gate_mlp: bfloat16 [4096, 14336], P('kv', 'tp'), may hold values from -0.09375 to 0.09375
- w_up: bfloat16 [4096, 14336], P('kv', 'tp'), may hold values from -0.09375 to 0.09375
- w_down: bfloat16 [14336, 4096], P('tp', 'kv'), may hold values from -0.0625 to 0.0625
Outputs:
- result: bfloat16 [640, 4096], P('grp', ('kv', 'tp')), parts along dimension 0
- new_memory: float32 [640, 16, 128, 128], P(('grp', 'kv'), 'tp'), parts along dimension 0
There are 2 independent parts, one for each index of `grp`. A program takes and returns all parts, laid end to end along the dimension named above; an argument that names none is the same for every part. Nothing has to cross between parts.
Inputs may be any that keep to these rules, and one draw needn't show every extreme that they name: Within each part along grp the lengths sum to 1310720 and the longest is exactly 16384.
All inputs are finite; a program needn't handle non-finite values. No bound on the sum of `lengths` on one device may be relied on, other than what follows from the above.
Results may differ from a plain program's by a relative error of at most 0.025.
Values may be sent and summed in bfloat16 or wider, within the bound.
No kernel may reach another device: no remote copies, remote signals or barrier semaphores. Data moves between devices by JAX's collectives and lax.ppermute only.
A program may use at most 64 MiB of HBM per device.

v0:
```python
import jax
import jax.numpy as jnp
from jax import lax
from jax.sharding import PartitionSpec as P

D = 4096
HEADS = 16
epsilon = 1e-06


def from_everyone(array, axis):
    copies = jnp.broadcast_to(array, (lax.axis_size(axis), *array.shape))
    return lax.all_to_all(copies, axis, split_axis=0, concat_axis=0, tiled=True)


def taken_together(array, axis):
    everything = from_everyone(array, axis)
    return jnp.sum(everything, axis=0)


def in_blocks(array, dim, size):
    lengths = array.shape
    pieces = array.reshape(*lengths[:dim], size, lengths[dim] // size, *lengths[dim + 1 :])
    return jnp.moveaxis(pieces, dim, 0)


def sum_at_owner(array, axis, dim):
    size = lax.axis_size(axis)
    pieces = lax.all_to_all(in_blocks(array, dim, size), axis, 0, 0, tiled=True)
    return jnp.sum(pieces.astype(jnp.float32), axis=0)


def rotate(values, position):
    half_width = values.shape[-1] // 2
    inverse = 10000.0 ** (-jnp.arange(half_width, dtype=jnp.float32) / half_width)
    angles = position[:, None] * inverse[None, :]
    cosine = jnp.cos(angles)[:, None, :]
    sine = jnp.sin(angles)[:, None, :]
    first = values[..., :half_width]
    second = values[..., half_width:]
    return jnp.concatenate(
        [first * cosine - second * sine, second * cosine + first * sine], axis=-1
    )


def head_decay(head_index):
    exponent = -5.0 - head_index.astype(jnp.float32) * (7.0 / max(HEADS - 1, 1))
    return 1.0 - jnp.exp2(exponent)


def retain(memory, queries, key_rows, value_rows, gate_rows, head_gain, decay_rate):
    new_memory = (
        decay_rate[None, :, None, None] * memory
        + key_rows[:, :, :, None] * value_rows[:, :, None, :]
    )
    readout = jnp.einsum(
        "bhd,bhde->bhe",
        queries * queries.shape[-1] ** (-0.5),
        new_memory,
        precision=lax.Precision.HIGHEST,
    )
    centred = readout - jnp.mean(readout, axis=-1, keepdims=True)
    normed = centred * lax.rsqrt(jnp.mean(centred * centred, axis=-1, keepdims=True) + epsilon)
    normed = normed.reshape(readout.shape[0], -1) * head_gain.astype(jnp.float32)
    return (new_memory, (normed * jax.nn.silu(gate_rows)).astype(jnp.bfloat16))


def per_device(
    tokens,
    lengths,
    memory,
    norm_attn,
    w_query,
    w_key,
    w_value,
    w_gate,
    head_gain,
    w_out,
    norm_mlp,
    w_gate_mlp,
    w_up,
    w_down,
):
    own_count = memory.shape[0]
    heads_local = memory.shape[1]
    head_size = memory.shape[2]
    width_local = w_query.shape[1]
    gathered = lax.all_gather(tokens, "tp", axis=1, tiled=True)
    tok_float = gathered.astype(jnp.float32)
    square_part = jnp.sum(tok_float * tok_float, axis=1)
    scaled = (tok_float * norm_attn.astype(jnp.float32)).astype(jnp.bfloat16)
    own_start = lax.axis_index("kv") * own_count
    square_total = taken_together(square_part, "kv")
    own_squares = lax.dynamic_slice_in_dim(square_total, own_start, own_count, 0)
    block_rows = scaled
    projected = sum_at_owner(
        jnp.concatenate(
            [
                jnp.dot(block_rows, weight, preferred_element_type=jnp.float32)
                for weight in (w_query, w_key, w_value, w_gate)
            ],
            axis=1,
        ).astype(jnp.bfloat16),
        "kv",
        0,
    )
    projected = projected * lax.rsqrt(own_squares / D + epsilon)[:, None]
    position = lengths.astype(jnp.float32)
    queries = rotate(
        projected[:, :width_local].reshape(own_count, heads_local, head_size), position
    )
    key_rows = rotate(
        projected[:, width_local : 2 * width_local].reshape(own_count, heads_local, head_size),
        position,
    )
    value_rows = projected[:, 2 * width_local : 3 * width_local].reshape(
        own_count, heads_local, head_size
    )
    gate_rows = projected[:, 3 * width_local :]
    decay_rate = head_decay(lax.axis_index("tp") * heads_local + jnp.arange(heads_local))
    new_memory, mixed = retain(
        memory, queries, key_rows, value_rows, gate_rows, head_gain, decay_rate
    )
    attn_part = jnp.dot(
        lax.all_gather(mixed, "kv", axis=0, tiled=True), w_out, preferred_element_type=jnp.float32
    )
    attn_total = sum_at_owner(attn_part.astype(jnp.bfloat16), "tp", 1)
    middle = (tokens.astype(jnp.float32) + attn_total).astype(jnp.bfloat16)
    mid_float = middle.astype(jnp.float32)
    gathered_mid = lax.all_gather(middle, "tp", axis=1, tiled=True)
    gathered_float = gathered_mid.astype(jnp.float32)
    mid_squares = jnp.sum(gathered_float * gathered_float, axis=1)
    scaled_mid = (gathered_float * norm_mlp.astype(jnp.float32)).astype(jnp.bfloat16)
    ff_local = w_up.shape[1]
    pieces = 1
    span = scaled_mid.shape[0] // pieces
    own_span = span // lax.axis_size("kv")
    span_start = lax.axis_index("kv") * own_span
    square_sums = taken_together(mid_squares, "kv")
    span_squares = lax.dynamic_slice_in_dim(square_sums, span_start, own_span, 0)
    block_rows = scaled_mid
    both_terms = lax.psum_scatter(
        jnp.concatenate(
            [
                jnp.dot(block_rows, w_gate_mlp, preferred_element_type=jnp.float32),
                jnp.dot(block_rows, w_up, preferred_element_type=jnp.float32),
            ],
            axis=1,
        ).astype(jnp.bfloat16),
        "kv",
        scatter_dimension=0,
        tiled=True,
    ).astype(jnp.float32)
    inv_mlp = lax.rsqrt(span_squares / D + epsilon)[:, None]
    gate_mlp = inv_mlp * both_terms[:, :ff_local]
    up_rows = inv_mlp * both_terms[:, ff_local:]
    hidden = (jax.nn.silu(gate_mlp) * up_rows).astype(jnp.bfloat16)
    partial_mlp = jnp.dot(
        lax.all_gather(hidden, "kv", axis=0, tiled=True), w_down, preferred_element_type=jnp.float32
    )
    results = sum_at_owner(partial_mlp.astype(jnp.bfloat16), "tp", 1)
    return ((mid_float + results).astype(jnp.bfloat16), new_memory)


def solution(mesh):
    in_specs = (
        P("grp", ("kv", "tp")),
        P(("grp", "kv")),
        P(("grp", "kv"), "tp", None, None),
        P("kv"),
        P("kv", "tp"),
        P("kv", "tp"),
        P("kv", "tp"),
        P("kv", "tp"),
        P("tp"),
        P("tp", "kv"),
        P("kv"),
        P("kv", "tp"),
        P("kv", "tp"),
        P("tp", "kv"),
    )
    out_specs = (P("grp", ("kv", "tp")), P(("grp", "kv"), "tp", None, None))
    return jax.shard_map(
        per_device, mesh=mesh, in_specs=in_specs, out_specs=out_specs, check_vma=False
    )
```

profile of v0, /device:TPU:65, one launch (start us, length us, event | category | flops | bytes accessed | tf_op | source)
XLA Modules:
  0.0 281.9 jit_solution(7506747860716999850)
XLA Ops:
  0.6 0.0 copy-start
  0.7 56.5 %all_gather.12 = bf16[320,256]{0,1:T(8,128)(2,1)S(1)} all-gather(bf16[320,16]{0,1:T(8,128)(2,1)} %param.14), channel_id=1, replica_groups=mesh['grp'=2,'kv'=16,'tp'=16] {'tp'}, dimensions={1}, use_global_device_ids=true | all-gather | bytes 174080 | tf_op jit(solution)/shard_map/all_gather | solution.py:88
  57.1 0.1 fusion.4
  57.2 0.6 broadcast_in_dim.4
  57.8 7.1 %all-to-all-start.1 = ((f32[16,1,320]{2,1,0:T(1,128)}), f32[16,1,320]{2,1,0:T(1,128)S(1)}, u32[]{:S(2)}, u32[]{:S(2)}) async-start(f32[16,1,320]{2,1,0:T(1,128)} %broadcast_in_dim.4), calls=%async_computation.1 | async-start | bytes 49152 | tf_op jit(solution)/shard_map/all_to_all | solution.py:13
  64.9 0.7 convert_element_type.69
  65.6 1.1 convolution_convert_fusion.6
  66.8 1.2 convolution_convert_fusion.5
  68.0 0.0 copy-start.9
  68.0 0.0 copy-start.10
  68.0 0.3 convolution_convert_fusion.4
  68.3 0.3 convolution_convert_fusion.7
  68.7 0.0 copy-start.2
  68.7 0.8 pad_maximum_fusion.1
  69.5 6.7 %all-to-all-done.1 = f32[16,1,320]{2,1,0:T(1,128)S(1)} async-done(((f32[16,1,320]{2,1,0:T(1,128)}), f32[16,1,320]{2,1,0:T(1,128)S(1)}, u32[]{:S(2)}, u32[]{:S(2)}) %all-to-all-start.1) | async-done | bytes 20512 | tf_op jit(solution)/shard_map/all_to_all | solution.py:13
  76.2 4.7 %all-to-all-start = ((bf16[16,20,512]{2,1,0:T(8,128)(2,1)}), bf16[16,20,512]{2,1,0:T(8,128)(2,1)S(1)}, u32[]{:S(2)}, u32[]{:S(2)}) async-start(bf16[16,20,512]{2,1,0:T(8,128)(2,1)} %pad_maximum_fusion.1), calls=%async_computation | async-start | bytes 786432 | tf_op jit(solution)/shard_map/all_to_all | solution.py:29
  81.1 0.1 add_rsqrt_fusion.2
  81.2 17.7 %all-to-all-done = bf16[16,20,512]{2,1,0:T(8,128)(2,1)S(1)} async-done(((bf16[16,20,512]{2,1,0:T(8,128)(2,1)}), bf16[16,20,512]{2,1,0:T(8,128)(2,1)S(1)}, u32[]{:S(2)}, u32[]{:S(2)}) %all-to-all-start) | async-done | bytes 327712 | tf_op jit(solution)/shard_map/all_to_all | solution.py:29
  98.9 0.1 convert_reduce_fusion
  99.0 0.1 broadcast_multiply_fusion
  99.0 0.1 fusion.21
  99.2 0.1 fusion.26
  99.3 0.1 maximum_bitcast_fusion
  99.3 0.4 multiply_add_fusion
  99.8 0.0 copy-start.1
  99.8 0.0 copy-start.5
  99.8 0.0 copy-start.11
  99.8 0.0 copy-start.8
  99.8 1.2 fusion.1
  101.0 0.1 bitcast_reduce_fusion
  101.1 0.2 multiply_reduce_fusion
  101.3 0.1 fusion.28
  101.4 26.0 %all-gather = bf16[16,20,128]{2,1,0:T(8,128)(2,1)S(1)} all-gather(bf16[1,20,128]{2,1,0:T(8,128)(2,1)S(1)} %fusion.28), channel_id=1, replica_groups=mesh['grp'=2,'kv'=16,'tp'=16] {'kv'}, dimensions={0}, use_global_device_ids=true | all-gather | bytes 87040 | tf_op jit(solution)/shard_map/all_gather | solution.py:125
  127.4 0.2 convolution_convert_fusion.3
  127.6 0.0 copy-start.3
  127.6 0.8 copy.23
  128.4 15.3 %all-to-all-start.2 = ((bf16[16,320,16]{1,2,0:T(8,128)(2,1)}), bf16[16,320,16]{1,2,0:T(8,128)(2,1)S(1)}, u32[]{:S(2)}, u32[]{:S(2)}) async-start(bf16[16,320,16]{1,2,0:T(8,128)(2,1)} %bitcast.10), calls=%async_computation.2 | async-start | bytes 393216 | tf_op jit(solution)/shard_map/all_to_all | solution.py:29
  143.7 1.3 dynamic-slice.4
  145.7 8.3 %all-to-all-done.2 = bf16[16,320,16]{1,2,0:T(8,128)(2,1)S(1)} async-done(((bf16[16,320,16]{1,2,0:T(8,128)(2,1)}), bf16[16,320,16]{1,2,0:T(8,128)(2,1)S(1)}, u32[]{:S(2)}, u32[]{:S(2)}) %all-to-all-start.2) | async-done | bytes 163872 | tf_op jit(solution)/shard_map/all_to_all | solution.py:29
  154.0 15.1 %all_gather.14 = bf16[320,256]{0,1:T(8,128)(2,1)S(1)} all-gather(bf16[320,16]{0,1:T(8,128)(2,1)S(1)} %add_convert_fusion.1), channel_id=1, replica_groups=mesh['grp'=2,'kv'=16,'tp'=16] {'tp'}, dimensions={1}, use_global_device_ids=true | all-gather | bytes 174080 | tf_op jit(solution)/shard_map/all_gather | solution.py:130
  169.1 0.1 fusion.5
  169.1 0.6 broadcast_in_dim.5
  169.8 4.7 %all-to-all-start.3 = ((f32[16,1,320]{2,1,0:T(1,128)}), f32[16,1,320]{2,1,0:T(1,128)S(1)}, u32[]{:S(2)}, u32[]{:S(2)}) async-start(f32[16,1,320]{2,1,0:T(1,128)} %broadcast_in_dim.5), calls=%async_computation.3 | async-start | bytes 49152 | tf_op jit(solution)/shard_map/all_to_all | solution.py:13
  174.4 0.4 convolution_convert_fusion
  174.9 0.4 convolution_convert_fusion.1
  175.3 0.1 pad_maximum_fusion
  175.4 32.2 %fusion = bf16[24,1792]{1,0:T(8,128)(2,1)S(1)} fusion(bf16[320,1792]{1,0:T(8,128)(2,1)S(1)} %pad_maximum_fusion), kind=kCustom, calls=%all-reduce-scatter | all-reduce-scatter fusion | flops 688129 | bytes 1234944
  207.6 2.7 collective-permute-start.1
  210.3 2.9 %collective-permute-start = (bf16[24,1792]{1,0:T(8,128)(2,1)S(1)}, bf16[24,1792]{1,0:T(8,128)(2,1)S(1)}, u32[]{:S(2)}, u32[]{:S(2)}) collective-permute-start(bf16[24,1792]{1,0:T(8,128)(2,1)S(1)} %fusion), channel_id=1, source_target_pairs={{0,16},{16,32},{32,48},{48,64},{64,80},{80,96},{96,112},{112,128},... | collective-permute-start | bytes 258056
  213.3 5.5 %collective-permute-start.2 = (bf16[12,1792]{1,0:T(8,128)(2,1)S(1)}, bf16[12,1792]{1,0:T(8,128)(2,1)S(1)}, u32[]{:S(2)}, u32[]{:S(2)}) collective-permute-start(bf16[12,1792]{1,0:T(8,128)(2,1)S(1)} %slice.50), channel_id=1, source_target_pairs={{0,48},{16,64},{32,80},{48,96},{64,112},{80,128},{96,144},{112,160... | collective-permute-start | bytes 129032
  218.8 0.0 all-to-all-done.3
  218.9 0.1 add_rsqrt_fusion
  218.9 1.1 collective-permute-done.2
  220.0 0.0 collective-permute-done.1
  220.0 0.0 collective-permute-done
  220.1 0.6 concatenate.40
  220.6 0.0 copy-start.4
  220.7 0.1 fusion.11
  220.8 28.5 %all-gather.1 = bf16[16,20,896]{2,1,0:T(8,128)(2,1)S(1)} all-gather(bf16[1,20,896]{2,1,0:T(8,128)(2,1)S(1)} %fusion.11), channel_id=1, replica_groups=mesh['grp'=2,'kv'=16,'tp'=16] {'kv'}, dimensions={0}, use_global_device_ids=true | all-gather | bytes 609280 | tf_op jit(solution)/shard_map/all_gather | solution.py:159
  249.3 0.1 reshape.198
  249.5 0.3 convolution_convert_fusion.2
  249.8 0.2 copy.25
  250.0 31.3 %all_to_all.27 = bf16[16,320,16]{1,2,0:T(8,128)(2,1)S(1)} all-to-all(bf16[16,320,16]{1,2,0:T(8,128)(2,1)S(1)} %bitcast.47), channel_id=1, replica_groups=mesh['grp'=2,'kv'=16,'tp'=16] {'tp'}, dimensions={0} | all-to-all | bytes 327680 | tf_op jit(solution)/shard_map/all_to_all | solution.py:29
  281.3 0.6 add_convert_fusion
  (33 shorter events, 0.4 us)
Async XLA Ops:
  0.6 173.8 %copy-start = (bf16[256,896]{1,0:T(8,128)(2,1)S(1)}, bf16[256,896]{1,0:T(8,128)(2,1)}, u32[]{:S(2)}) copy-start(bf16[256,896]{1,0:T(8,128)(2,1)} %param.26) | copy-start | bytes 1376260
  0.6 67.3 %copy-start.6 = (bf16[256,128]{1,0:T(8,128)(2,1)S(1)}, bf16[256,128]{1,0:T(8,128)(2,1)}, u32[]{:S(2)}) copy-start(bf16[256,128]{1,0:T(8,128)(2,1)} %param.21) | copy-start | bytes 196612
  0.7 67.7 %copy-start.7 = (bf16[256,128]{1,0:T(8,128)(2,1)S(1)}, bf16[256,128]{1,0:T(8,128)(2,1)}, u32[]{:S(2)}) copy-start(bf16[256,128]{1,0:T(8,128)(2,1)} %param.18) | copy-start | bytes 196612
  57.8 18.4 %all-to-all-start.1 = ((f32[16,1,320]{2,1,0:T(1,128)}), f32[16,1,320]{2,1,0:T(1,128)S(1)}, u32[]{:S(2)}, u32[]{:S(2)}) async-start(f32[16,1,320]{2,1,0:T(1,128)} %broadcast_in_dim.4), calls=%async_computation.1 | async-start | bytes 49152 | tf_op jit(solution)/shard_map/all_to_all | solution.py:13
  68.0 13.1 %copy-start.9 = (s32[20]{0:T(128)S(1)}, s32[20]{0:T(128)}, u32[]{:S(2)}) copy-start(s32[20]{0:T(128)} %param.15) | copy-start | bytes 244
  68.0 13.1 %copy-start.10 = (bf16[128]{0:T(256)(128)(2,1)S(1)}, bf16[128]{0:T(256)(128)(2,1)}, u32[]{:S(2)}) copy-start(bf16[128]{0:T(256)(128)(2,1)} %param.22) | copy-start | bytes 772
  68.7 30.7 %copy-start.2 = (f32[20,1,128,128]{3,2,1,0:T(8,128)S(1)}, f32[20,1,128,128]{3,2,1,0:T(8,128)}, u32[]{:S(2)}) copy-start(f32[20,1,128,128]{3,2,1,0:T(8,128)} %param.16) | copy-start | bytes 3932164
  76.2 22.7 %all-to-all-start = ((bf16[16,20,512]{2,1,0:T(8,128)(2,1)}), bf16[16,20,512]{2,1,0:T(8,128)(2,1)S(1)}, u32[]{:S(2)}, u32[]{:S(2)}) async-start(bf16[16,20,512]{2,1,0:T(8,128)(2,1)} %pad_maximum_fusion.1), calls=%async_computation | async-start | bytes 786432 | tf_op jit(solution)/shard_map/all_to_all | solution.py:29
  99.8 28.7 %copy-start.1 = (f32[20,1,128,128]{3,2,1,0:T(8,128)}, f32[20,1,128,128]{3,2,1,0:T(8,128)S(1)}, u32[]{:S(2)}) copy-start(f32[20,1,128,128]{3,2,1,0:T(8,128)S(1)} %multiply_add_fusion) | copy-start | bytes 3932164
  99.8 27.6 %copy-start.5 = (bf16[128,256]{1,0:T(8,128)(2,1)S(1)}, bf16[128,256]{1,0:T(8,128)(2,1)}, u32[]{:S(2)}) copy-start(bf16[128,256]{1,0:T(8,128)(2,1)} %param.23) | copy-start | bytes 196612
  99.8 43.9 %copy-start.11 = (bf16[256]{0:T(256)(128)(2,1)S(1)}, bf16[256]{0:T(256)(128)(2,1)}, u32[]{:S(2)}) copy-start(bf16[256]{0:T(256)(128)(2,1)} %param.24) | copy-start | bytes 1540
  99.8 54.2 %copy-start.8 = (bf16[320,16]{0,1:T(8,128)(2,1)S(1)}, bf16[320,16]{0,1:T(8,128)(2,1)}, u32[]{:S(2)}) copy-start(bf16[320,16]{0,1:T(8,128)(2,1)} %param.14) | copy-start | bytes 30724
  127.6 47.3 %copy-start.3 = (bf16[256,896]{1,0:T(8,128)(2,1)S(1)}, bf16[256,896]{1,0:T(8,128)(2,1)}, u32[]{:S(2)}) copy-start(bf16[256,896]{1,0:T(8,128)(2,1)} %param.25) | copy-start | bytes 1376260
  128.4 25.5 %all-to-all-start.2 = ((bf16[16,320,16]{1,2,0:T(8,128)(2,1)}), bf16[16,320,16]{1,2,0:T(8,128)(2,1)S(1)}, u32[]{:S(2)}, u32[]{:S(2)}) async-start(bf16[16,320,16]{1,2,0:T(8,128)(2,1)} %bitcast.10), calls=%async_computation.2 | async-start | bytes 393216 | tf_op jit(solution)/shard_map/all_to_all | solution.py:29
  169.8 49.1 %all-to-all-start.3 = ((f32[16,1,320]{2,1,0:T(1,128)}), f32[16,1,320]{2,1,0:T(1,128)S(1)}, u32[]{:S(2)}, u32[]{:S(2)}) async-start(f32[16,1,320]{2,1,0:T(1,128)} %broadcast_in_dim.5), calls=%async_computation.3 | async-start | bytes 49152 | tf_op jit(solution)/shard_map/all_to_all | solution.py:13
  207.6 12.4 %collective-permute-start.1 = (bf16[24,1792]{1,0:T(8,128)(2,1)S(1)}, bf16[24,1792]{1,0:T(8,128)(2,1)S(1)}, u32[]{:S(2)}, u32[]{:S(2)}) collective-permute-start(bf16[24,1792]{1,0:T(8,128)(2,1)S(1)} %fusion), channel_id=1, source_target_pairs={{0,32},{16,48},{32,64},{48,80},{64,96},{80,112},{96,128},{112,144}... | collective-permute-start | bytes 258056
  210.3 9.7 %collective-permute-start = (bf16[24,1792]{1,0:T(8,128)(2,1)S(1)}, bf16[24,1792]{1,0:T(8,128)(2,1)S(1)}, u32[]{:S(2)}, u32[]{:S(2)}) collective-permute-start(bf16[24,1792]{1,0:T(8,128)(2,1)S(1)} %fusion), channel_id=1, source_target_pairs={{0,16},{16,32},{32,48},{48,64},{64,80},{80,96},{96,112},{112,128},... | collective-permute-start | bytes 258056
  213.3 6.8 %collective-permute-start.2 = (bf16[12,1792]{1,0:T(8,128)(2,1)S(1)}, bf16[12,1792]{1,0:T(8,128)(2,1)S(1)}, u32[]{:S(2)}, u32[]{:S(2)}) collective-permute-start(bf16[12,1792]{1,0:T(8,128)(2,1)S(1)} %slice.50), channel_id=1, source_target_pairs={{0,48},{16,64},{32,80},{48,96},{64,112},{80,128},{96,144},{112,160... | collective-permute-start | bytes 129032
  220.6 28.8 %copy-start.4 = (bf16[896,256]{1,0:T(8,128)(2,1)S(1)}, bf16[896,256]{1,0:T(8,128)(2,1)}, u32[]{:S(2)}) copy-start(bf16[896,256]{1,0:T(8,128)(2,1)} %param.27) | copy-start | bytes 1376260
where the time goes:
time: 283 us; the launch traced here: 282 us
  blocking collectives  190 us (67%)
  starting transfers between devices  42.9 us (15%)
  waiting for transfers between devices  33.8 us (12%)
  matrix products  5.51 us (2%)
  local copies, waits for them, and re-layouts  4.37 us (2%)
  other arithmetic  4 us (1%)
    all_gather x1, blocking collectives, per_device(): gathered = lax.all_gather(tokens, 'tp', axis=1, tiled=True)  56.5 us
    unnamed x1, blocking collectives  32.2 us
    all_to_all x1, blocking collectives, sum_at_owner(): pieces = lax.all_to_all(in_blocks(array, dim, size), axis, 0, 0, tiled=True)  31.3 us
    all_gather x1, blocking collectives, per_device(): lax.all_gather(hidden, 'kv', axis=0, tiled=True)  28.5 us
    all_gather x1, blocking collectives, per_device(): lax.all_gather(mixed, 'kv', axis=0, tiled=True)  26 us
    all_to_all x2, waiting for transfers between devices, sum_at_owner(): pieces = lax.all_to_all(in_blocks(array, dim, size), axis, 0, 0, tiled=True)  25.9 us
    all_to_all x2, starting transfers between devices, sum_at_owner(): pieces = lax.all_to_all(in_blocks(array, dim, size), axis, 0, 0, tiled=True)  20 us
    all_gather x1, blocking collectives, per_device(): gathered_mid = lax.all_gather(middle, 'tp', axis=1, tiled=True)  15.1 us
  transfers between devices with their start and end apart: 7, of which 4 were waited for; matrix products, arithmetic and copies ran while one was open for 14% of the time, Pallas kernels for 0%

commit v1 on v0

--- a/solution.py
+++ b/solution.py
@@ -122,7 +122,11 @@
         memory, queries, key_rows, value_rows, gate_rows, head_gain, decay_rate
     )
     attn_part = jnp.dot(
-        lax.all_gather(mixed, "kv", axis=0, tiled=True), w_out, preferred_element_type=jnp.float32
+        jnp.concatenate(
+            lax.all_to_all(jnp.stack([mixed] * lax.axis_size("kv")), "kv", 0, 0), axis=0
+        ),
+        w_out,
+        preferred_element_type=jnp.float32,
     )
     attn_total = sum_at_owner(attn_part.astype(jnp.bfloat16), "tp", 1)
     middle = (tokens.astype(jnp.float32) + attn_total).astype(jnp.bfloat16)

time: 283 us -> 269 us (0.951)
  starting transfers between devices: 42.9 us -> 33.8 us
  blocking collectives: 190 us -> 185 us
    all_gather x1 -> x0, blocking collectives: 26 us -> none  [per_device(): lax.all_gather(mixed, 'kv', axis=0, tiled=True)]
    all_to_all x0 -> x1, blocking collectives: none -> 23 us  [per_device(): lax.all_to_all(jnp.stack([mixed] * lax.axis_size('kv')), 'kv', 0, 0)]
    all_to_all x2, starting transfers between devices: 20 us -> 11.9 us  [sum_at_owner(): pieces = lax.all_to_all(in_blocks(array, dim, size), axis, 0, 0, tiled=True)]
  transfers between devices with their start and end apart: 7 -> 7, of which waited for: 4 -> 4; matrix products, arithmetic and copies ran while one was open for 14% -> 15% of each run, Pallas kernels for 0% -> 0%
where the time goes in v1:
time: 269 us
  blocking collectives  185 us (69%)
  starting transfers between devices  33.8 us (13%)
  waiting for transfers between devices  33.8 us (13%)
  matrix products  5.51 us (2%)
  local copies, waits for them, and re-layouts  4.39 us (2%)
  other arithmetic  4 us (1%)
    all_gather x1, blocking collectives, per_device(): gathered = lax.all_gather(tokens, 'tp', axis=1, tiled=True)  56.5 us
    unnamed x1, blocking collectives  32.1 us
    all_to_all x1, blocking collectives, sum_at_owner(): pieces = lax.all_to_all(in_blocks(array, dim, size), axis, 0, 0, tiled=True)  31.5 us
    all_gather x1, blocking collectives, per_device(): lax.all_gather(hidden, 'kv', axis=0, tiled=True)  27.3 us
    all_to_all x2, waiting for transfers between devices, sum_at_owner(): pieces = lax.all_to_all(in_blocks(array, dim, size), axis, 0, 0, tiled=True)  25.9 us
    all_to_all x1, blocking collectives, per_device(): lax.all_to_all(jnp.stack([mixed] * lax.axis_size('kv')), 'kv', 0, 0)  23 us
    all_gather x1, blocking collectives, per_device(): gathered_mid = lax.all_gather(middle, 'tp', axis=1, tiled=True)  15.1 us
    all_to_all x2, starting transfers between devices, sum_at_owner(): pieces = lax.all_to_all(in_blocks(array, dim, size), axis, 0, 0, tiled=True)  11.9 us
  transfers between devices with their start and end apart: 7, of which 4 were waited for; matrix products, arithmetic and copies ran while one was open for 15% of the time, Pallas kernels for 0%

profile of v1, /device:TPU:65, one launch (start us, length us, event | category | flops | bytes accessed | tf_op | source)
XLA Modules:
  0.0 268.7 jit_solution(4043496603325899727)
XLA Ops:
  0.6 0.0 copy-start
  0.7 56.5 %all_gather.9 = bf16[320,256]{0,1:T(8,128)(2,1)S(1)} all-gather(bf16[320,16]{0,1:T(8,128)(2,1)} %param.14), channel_id=1, replica_groups=mesh['grp'=2,'kv'=16,'tp'=16] {'tp'}, dimensions={1}, use_global_device_ids=true | all-gather | bytes 174080 | tf_op jit(solution)/shard_map/all_gather | solution.py:88
  57.1 0.1 fusion.4
  57.2 0.6 broadcast_in_dim.4
  57.8 7.1 %all-to-all-start.1 = ((f32[16,1,320]{2,1,0:T(1,128)}), f32[16,1,320]{2,1,0:T(1,128)S(1)}, u32[]{:S(2)}, u32[]{:S(2)}) async-start(f32[16,1,320]{2,1,0:T(1,128)} %broadcast_in_dim.4), calls=%async_computation.1 | async-start | bytes 49152 | tf_op jit(solution)/shard_map/all_to_all | solution.py:13
  64.9 0.7 convert_element_type.69
  65.6 1.1 convolution_convert_fusion.6
  66.8 1.2 convolution_convert_fusion.5
  68.0 0.0 copy-start.9
  68.0 0.0 copy-start.10
  68.0 0.3 convolution_convert_fusion.4
  68.3 0.3 convolution_convert_fusion.7
  68.7 0.0 copy-start.2
  68.7 0.8 pad_maximum_fusion.1
  69.5 6.7 %all-to-all-done.1 = f32[16,1,320]{2,1,0:T(1,128)S(1)} async-done(((f32[16,1,320]{2,1,0:T(1,128)}), f32[16,1,320]{2,1,0:T(1,128)S(1)}, u32[]{:S(2)}, u32[]{:S(2)}) %all-to-all-start.1) | async-done | bytes 20512 | tf_op jit(solution)/shard_map/all_to_all | solution.py:13
  76.2 4.7 %all-to-all-start = ((bf16[16,20,512]{2,1,0:T(8,128)(2,1)}), bf16[16,20,512]{2,1,0:T(8,128)(2,1)S(1)}, u32[]{:S(2)}, u32[]{:S(2)}) async-start(bf16[16,20,512]{2,1,0:T(8,128)(2,1)} %pad_maximum_fusion.1), calls=%async_computation | async-start | bytes 786432 | tf_op jit(solution)/shard_map/all_to_all | solution.py:29
  81.1 0.1 add_rsqrt_fusion.2
  81.2 17.7 %all-to-all-done = bf16[16,20,512]{2,1,0:T(8,128)(2,1)S(1)} async-done(((bf16[16,20,512]{2,1,0:T(8,128)(2,1)}), bf16[16,20,512]{2,1,0:T(8,128)(2,1)S(1)}, u32[]{:S(2)}, u32[]{:S(2)}) %all-to-all-start) | async-done | bytes 327712 | tf_op jit(solution)/shard_map/all_to_all | solution.py:29
  98.9 0.1 convert_reduce_fusion
  99.0 0.1 broadcast_multiply_fusion
  99.0 0.1 fusion.21
  99.2 0.1 fusion.26
  99.3 0.1 maximum_bitcast_fusion
  99.3 0.4 multiply_add_fusion
  99.8 0.0 copy-start.1
  99.8 0.0 copy-start.5
  99.8 0.0 copy-start.11
  99.8 0.0 copy-start.8
  99.8 1.2 fusion.1
  101.0 0.1 bitcast_reduce_fusion
  101.1 0.2 multiply_reduce_fusion
  101.3 0.1 multiply_convert_fusion
  101.4 23.0 %all_to_all.32 = bf16[16,20,128]{2,1,0:T(8,128)(2,1)S(1)} all-to-all(bf16[16,20,128]{2,1,0:T(8,128)(2,1)S(1)} %stack.2), channel_id=1, replica_groups=mesh['grp'=2,'kv'=16,'tp'=16] {'kv'}, dimensions={0} | all-to-all | bytes 163840 | tf_op jit(solution)/shard_map/all_to_all | solution.py:126
  124.5 0.2 convolution_convert_fusion.3
  124.7 0.0 copy-start.3
  124.7 0.8 copy.23
  125.5 7.1 %all-to-all-start.3 = ((bf16[16,320,16]{1,2,0:T(8,128)(2,1)}), bf16[16,320,16]{1,2,0:T(8,128)(2,1)S(1)}, u32[]{:S(2)}, u32[]{:S(2)}) async-start(bf16[16,320,16]{1,2,0:T(8,128)(2,1)} %bitcast.9), calls=%async_computation.3 | async-start | bytes 393216 | tf_op jit(solution)/shard_map/all_to_all | solution.py:29
  132.6 1.3 dynamic-slice.4
  134.6 8.3 %all-to-all-done.3 = bf16[16,320,16]{1,2,0:T(8,128)(2,1)S(1)} async-done(((bf16[16,320,16]{1,2,0:T(8,128)(2,1)}), bf16[16,320,16]{1,2,0:T(8,128)(2,1)S(1)}, u32[]{:S(2)}, u32[]{:S(2)}) %all-to-all-start.3) | async-done | bytes 163872 | tf_op jit(solution)/shard_map/all_to_all | solution.py:29
  142.9 15.1 %all_gather.10 = bf16[320,256]{0,1:T(8,128)(2,1)S(1)} all-gather(bf16[320,16]{0,1:T(8,128)(2,1)S(1)} %add_convert_fusion.1), channel_id=1, replica_groups=mesh['grp'=2,'kv'=16,'tp'=16] {'tp'}, dimensions={1}, use_global_device_ids=true | all-gather | bytes 174080 | tf_op jit(solution)/shard_map/all_gather | solution.py:134
  158.0 0.1 fusion.5
  158.1 0.6 broadcast_in_dim.5
  158.7 3.9 %all-to-all-start.4 = ((f32[16,1,320]{2,1,0:T(1,128)}), f32[16,1,320]{2,1,0:T(1,128)S(1)}, u32[]{:S(2)}, u32[]{:S(2)}) async-start(f32[16,1,320]{2,1,0:T(1,128)} %broadcast_in_dim.5), calls=%async_computation.4 | async-start | bytes 49152 | tf_op jit(solution)/shard_map/all_to_all | solution.py:13
  162.6 0.4 convolution_convert_fusion
  163.1 0.4 convolution_convert_fusion.1
  163.5 0.1 pad_maximum_fusion
  163.6 32.1 %fusion = bf16[24,1792]{1,0:T(8,128)(2,1)S(1)} fusion(bf16[320,1792]{1,0:T(8,128)(2,1)S(1)} %pad_maximum_fusion), kind=kCustom, calls=%all-reduce-scatter | all-reduce-scatter fusion | flops 688129 | bytes 1234944
  195.7 2.3 collective-permute-start.1
  198.0 3.0 %collective-permute-start = (bf16[24,1792]{1,0:T(8,128)(2,1)S(1)}, bf16[24,1792]{1,0:T(8,128)(2,1)S(1)}, u32[]{:S(2)}, u32[]{:S(2)}) collective-permute-start(bf16[24,1792]{1,0:T(8,128)(2,1)S(1)} %fusion), channel_id=1, source_target_pairs={{0,16},{16,32},{32,48},{48,64},{64,80},{80,96},{96,112},{112,128},... | collective-permute-start | bytes 258056
  201.0 5.7 %collective-permute-start.2 = (bf16[12,1792]{1,0:T(8,128)(2,1)S(1)}, bf16[12,1792]{1,0:T(8,128)(2,1)S(1)}, u32[]{:S(2)}, u32[]{:S(2)}) collective-permute-start(bf16[12,1792]{1,0:T(8,128)(2,1)S(1)} %slice.50), channel_id=1, source_target_pairs={{0,48},{16,64},{32,80},{48,96},{64,112},{80,128},{96,144},{112,160... | collective-permute-start | bytes 129032
  206.7 0.0 all-to-all-done.4
  206.7 0.1 add_rsqrt_fusion
  206.8 1.1 collective-permute-done.2
  207.9 0.0 collective-permute-done.1
  207.9 0.0 collective-permute-done
  207.9 0.6 concatenate.40
  208.5 0.0 copy-start.4
  208.5 0.1 fusion.11
  208.6 27.3 %all-gather = bf16[16,20,896]{2,1,0:T(8,128)(2,1)S(1)} all-gather(bf16[1,20,896]{2,1,0:T(8,128)(2,1)S(1)} %fusion.11), channel_id=1, replica_groups=mesh['grp'=2,'kv'=16,'tp'=16] {'kv'}, dimensions={0}, use_global_device_ids=true | all-gather | bytes 609280 | tf_op jit(solution)/shard_map/all_gather | solution.py:163
  235.9 0.1 reshape.202
  236.0 0.3 convolution_convert_fusion.2
  236.4 0.2 copy.25
  236.5 31.5 %all_to_all.33 = bf16[16,320,16]{1,2,0:T(8,128)(2,1)S(1)} all-to-all(bf16[16,320,16]{1,2,0:T(8,128)(2,1)S(1)} %bitcast.43), channel_id=1, replica_groups=mesh['grp'=2,'kv'=16,'tp'=16] {'tp'}, dimensions={0} | all-to-all | bytes 327680 | tf_op jit(solution)/shard_map/all_to_all | solution.py:29
  268.1 0.6 add_convert_fusion
  (34 shorter events, 0.4 us)
Async XLA Ops:
  0.6 162.0 %copy-start = (bf16[256,896]{1,0:T(8,128)(2,1)S(1)}, bf16[256,896]{1,0:T(8,128)(2,1)}, u32[]{:S(2)}) copy-start(bf16[256,896]{1,0:T(8,128)(2,1)} %param.26) | copy-start | bytes 1376260
  0.6 67.3 %copy-start.6 = (bf16[256,128]{1,0:T(8,128)(2,1)S(1)}, bf16[256,128]{1,0:T(8,128)(2,1)}, u32[]{:S(2)}) copy-start(bf16[256,128]{1,0:T(8,128)(2,1)} %param.21) | copy-start | bytes 196612
  0.7 67.7 %copy-start.7 = (bf16[256,128]{1,0:T(8,128)(2,1)S(1)}, bf16[256,128]{1,0:T(8,128)(2,1)}, u32[]{:S(2)}) copy-start(bf16[256,128]{1,0:T(8,128)(2,1)} %param.18) | copy-start | bytes 196612
  57.8 18.4 %all-to-all-start.1 = ((f32[16,1,320]{2,1,0:T(1,128)}), f32[16,1,320]{2,1,0:T(1,128)S(1)}, u32[]{:S(2)}, u32[]{:S(2)}) async-start(f32[16,1,320]{2,1,0:T(1,128)} %broadcast_in_dim.4), calls=%async_computation.1 | async-start | bytes 49152 | tf_op jit(solution)/shard_map/all_to_all | solution.py:13
  68.0 13.1 %copy-start.9 = (s32[20]{0:T(128)S(1)}, s32[20]{0:T(128)}, u32[]{:S(2)}) copy-start(s32[20]{0:T(128)} %param.15) | copy-start | bytes 244
  68.0 13.1 %copy-start.10 = (bf16[128]{0:T(256)(128)(2,1)S(1)}, bf16[128]{0:T(256)(128)(2,1)}, u32[]{:S(2)}) copy-start(bf16[128]{0:T(256)(128)(2,1)} %param.22) | copy-start | bytes 772
  68.7 30.7 %copy-start.2 = (f32[20,1,128,128]{3,2,1,0:T(8,128)S(1)}, f32[20,1,128,128]{3,2,1,0:T(8,128)}, u32[]{:S(2)}) copy-start(f32[20,1,128,128]{3,2,1,0:T(8,128)} %param.16) | copy-start | bytes 3932164
  76.2 22.7 %all-to-all-start = ((bf16[16,20,512]{2,1,0:T(8,128)(2,1)}), bf16[16,20,512]{2,1,0:T(8,128)(2,1)S(1)}, u32[]{:S(2)}, u32[]{:S(2)}) async-start(bf16[16,20,512]{2,1,0:T(8,128)(2,1)} %pad_maximum_fusion.1), calls=%async_computation | async-start | bytes 786432 | tf_op jit(solution)/shard_map/all_to_all | solution.py:29
  99.8 25.7 %copy-start.1 = (f32[20,1,128,128]{3,2,1,0:T(8,128)}, f32[20,1,128,128]{3,2,1,0:T(8,128)S(1)}, u32[]{:S(2)}) copy-start(f32[20,1,128,128]{3,2,1,0:T(8,128)S(1)} %multiply_add_fusion) | copy-start | bytes 3932164
  99.8 24.7 %copy-start.5 = (bf16[128,256]{1,0:T(8,128)(2,1)S(1)}, bf16[128,256]{1,0:T(8,128)(2,1)}, u32[]{:S(2)}) copy-start(bf16[128,256]{1,0:T(8,128)(2,1)} %param.23) | copy-start | bytes 196612
  99.8 32.8 %copy-start.11 = (bf16[256]{0:T(256)(128)(2,1)S(1)}, bf16[256]{0:T(256)(128)(2,1)}, u32[]{:S(2)}) copy-start(bf16[256]{0:T(256)(128)(2,1)} %param.24) | copy-start | bytes 1540
  99.8 43.1 %copy-start.8 = (bf16[320,16]{0,1:T(8,128)(2,1)S(1)}, bf16[320,16]{0,1:T(8,128)(2,1)}, u32[]{:S(2)}) copy-start(bf16[320,16]{0,1:T(8,128)(2,1)} %param.14) | copy-start | bytes 30724
  124.7 38.4 %copy-start.3 = (bf16[256,896]{1,0:T(8,128)(2,1)S(1)}, bf16[256,896]{1,0:T(8,128)(2,1)}, u32[]{:S(2)}) copy-start(bf16[256,896]{1,0:T(8,128)(2,1)} %param.25) | copy-start | bytes 1376260
  125.5 17.3 %all-to-all-start.3 = ((bf16[16,320,16]{1,2,0:T(8,128)(2,1)}), bf16[16,320,16]{1,2,0:T(8,128)(2,1)S(1)}, u32[]{:S(2)}, u32[]{:S(2)}) async-start(bf16[16,320,16]{1,2,0:T(8,128)(2,1)} %bitcast.9), calls=%async_computation.3 | async-start | bytes 393216 | tf_op jit(solution)/shard_map/all_to_all | solution.py:29
  158.7 48.0 %all-to-all-start.4 = ((f32[16,1,320]{2,1,0:T(1,128)}), f32[16,1,320]{2,1,0:T(1,128)S(1)}, u32[]{:S(2)}, u32[]{:S(2)}) async-start(f32[16,1,320]{2,1,0:T(1,128)} %broadcast_in_dim.5), calls=%async_computation.4 | async-start | bytes 49152 | tf_op jit(solution)/shard_map/all_to_all | solution.py:13
  195.7 12.2 %collective-permute-start.1 = (bf16[24,1792]{1,0:T(8,128)(2,1)S(1)}, bf16[24,1792]{1,0:T(8,128)(2,1)S(1)}, u32[]{:S(2)}, u32[]{:S(2)}) collective-permute-start(bf16[24,1792]{1,0:T(8,128)(2,1)S(1)} %fusion), channel_id=1, source_target_pairs={{0,32},{16,48},{32,64},{48,80},{64,96},{80,112},{96,128},{112,144}... | collective-permute-start | bytes 258056
  198.0 9.9 %collective-permute-start = (bf16[24,1792]{1,0:T(8,128)(2,1)S(1)}, bf16[24,1792]{1,0:T(8,128)(2,1)S(1)}, u32[]{:S(2)}, u32[]{:S(2)}) collective-permute-start(bf16[24,1792]{1,0:T(8,128)(2,1)S(1)} %fusion), channel_id=1, source_target_pairs={{0,16},{16,32},{32,48},{48,64},{64,80},{80,96},{96,112},{112,128},... | collective-permute-start | bytes 258056
  201.0 6.9 %collective-permute-start.2 = (bf16[12,1792]{1,0:T(8,128)(2,1)S(1)}, bf16[12,1792]{1,0:T(8,128)(2,1)S(1)}, u32[]{:S(2)}, u32[]{:S(2)}) collective-permute-start(bf16[12,1792]{1,0:T(8,128)(2,1)S(1)} %slice.50), channel_id=1, source_target_pairs={{0,48},{16,64},{32,80},{48,96},{64,112},{80,128},{96,144},{112,160... | collective-permute-start | bytes 129032
  208.5 27.5 %copy-start.4 = (bf16[896,256]{1,0:T(8,128)(2,1)S(1)}, bf16[896,256]{1,0:T(8,128)(2,1)}, u32[]{:S(2)}) copy-start(bf16[896,256]{1,0:T(8,128)(2,1)} %param.27) | copy-start | bytes 1376260
